TPU v7x, 32 devices: a whole 2x2x4 slice. The times are simulated.
32 devices in a mesh: rep: 2 (over x), fs: 8 (over z, y), tp: 2 (over core).
Axes of the slice: x: 2, y: 2, z: 4, core: 2. Of those that a mesh axis runs over, the one named last changes fastest.
Arguments:
- inputs: bfloat16 [6144, 2048], P(('rep', 'fs')), may hold values from -6 to 6
- w_up: bfloat16 [2048, 4096], P('fs', 'tp'), may hold values from -0.125 to 0.125
- w_down: bfloat16 [4096, 2048], P('tp', 'fs'), may hold values from -0.09375 to 0.09375
- cotangent: bfloat16 [6144, 2048], P(('rep', 'fs')), may hold values from -6 to 6
Outputs:
- d_inputs: bfloat16 [6144, 2048], P(('rep', 'fs'))
- d_w_up: float32 [2048, 4096], P('fs', 'tp')
All inputs are finite; a program needn't handle non-finite values.
Results may differ from a plain program's by a relative error of at most 0.014.
Values may be sent and summed in bfloat16 or wider, within the bound.
A program may use at most 128 MiB of HBM per device.

v0:
```python
import jax
import jax.numpy as jnp
from jax import lax
from jax.sharding import PartitionSpec as P


def per_device(inputs, w_up, w_down, cotangent):
    n_rep = lax.axis_size("rep")
    rep = lax.axis_index("rep")
    tokens = inputs.shape[0]
    hidden = w_up.shape[1] // n_rep

    def from_rep(value, step):
        return lax.ppermute(value, "rep", [((r + step) % n_rep, r) for r in range(n_rep)])

    up_block = lax.dynamic_slice_in_dim(w_up, rep * hidden, hidden, axis=1)
    down_block = lax.dynamic_slice_in_dim(w_down, rep * hidden, hidden, axis=0)
    up_whole = lax.all_gather(up_block, "fs", axis=0, tiled=True)
    down_whole = lax.all_gather(down_block, "fs", axis=1, tiled=True)
    rows = jnp.concatenate([inputs] + [from_rep(inputs, k) for k in range(1, n_rep)], axis=0)
    cots = jnp.concatenate([cotangent] + [from_rep(cotangent, k) for k in range(1, n_rep)], axis=0)
    preact = jnp.dot(rows, up_whole, preferred_element_type=jnp.float32)
    grad_hidden = lax.dot_general(
        cots, down_whole, (((1,), (1,)), ((), ())), preferred_element_type=jnp.float32
    )
    grad_pre = (2.0 * jnp.maximum(preact, 0.0) * grad_hidden).astype(jnp.bfloat16)
    d_w = lax.dot_general(
        rows, grad_pre, (((0,), (0,)), ((), ())), preferred_element_type=jnp.float32
    ).astype(jnp.bfloat16)
    own_rows = lax.psum_scatter(d_w, "fs", scatter_dimension=0, tiled=True)
    partial_value = lax.dot_general(
        grad_pre, up_whole, (((1,), (1,)), ((), ())), preferred_element_type=jnp.float32
    )
    own = partial_value[:tokens]
    for k in range(1, n_rep):
        mine = partial_value[k * tokens : (k + 1) * tokens].astype(jnp.bfloat16)
        own = own + from_rep(mine, n_rep - k).astype(jnp.float32)
    d_inputs = lax.psum(own.astype(jnp.bfloat16), "tp")
    whole_rows = jnp.zeros((own_rows.shape[0], w_up.shape[1]), jnp.float32)
    for k in range(n_rep):
        block = own_rows if k == 0 else from_rep(own_rows, k)
        at = lax.rem(rep + k, n_rep) * hidden
        whole_rows = lax.dynamic_update_slice_in_dim(
            whole_rows, block.astype(jnp.float32), at, axis=1
        )
    return (d_inputs, whole_rows)


def solution(mesh):
    in_specs = (P(("rep", "fs"), None), P("fs", "tp"), P("tp", "fs"), P(("rep", "fs"), None))
    out_specs = (P(("rep", "fs"), None), P("fs", "tp"))
    return jax.shard_map(
        per_device, mesh=mesh, in_specs=in_specs, out_specs=out_specs, check_vma=False
    )
```

profile of v0, /device:TPU:0, one launch (start us, length us, event | category | flops | bytes accessed | tf_op | source)
XLA Modules:
  0.0 296.0 jit_solution(13149260380039072654)
XLA Ops:
  7.2 1.2 copy-done
  9.3 1.9 constant_dynamic-slice_fusion
  11.3 3.0 %collective-permute-start = (bf16[384,2048]{1,0:T(8,128)(2,1)S(1)}, bf16[384,2048]{1,0:T(8,128)(2,1)S(1)}, u32[]{:S(2)}, u32[]{:S(2)}) collective-permute-start(bf16[384,2048]{1,0:T(8,128)(2,1)S(1)} %copy-done.2), channel_id=1, source_target_pairs={{16,0},{0,16},{17,1},{1,17},{18,2},{2,18},{19,3},{3,19},{20,4},{4,... | collective-permute-start | bytes 4718600 | tf_op jit(solution)/shard_map/ppermute | solution.py:14
  14.4 1.3 constant_dynamic-update-slice_fusion.1
  15.7 33.8 %collective-permute-done = bf16[384,2048]{1,0:T(8,128)(2,1)S(1)} collective-permute-done((bf16[384,2048]{1,0:T(8,128)(2,1)S(1)}, bf16[384,2048]{1,0:T(8,128)(2,1)S(1)}, u32[]{:S(2)}, u32[]{:S(2)}) %collective-permute-start) | collective-permute-done | bytes 1572896 | tf_op jit(solution)/shard_map/ppermute | solution.py:14
  49.5 1.3 constant_dynamic-update-slice_fusion
  50.8 35.4 %all-gather.3.cloned.1.call-done = bf16[2048,1024]{1,0:T(8,128)(2,1)} async-done(((bf16[256,1024]{1,0:T(8,128)(2,1)}), bf16[2048,1024]{1,0:T(8,128)(2,1)}) %all-gather.3.cloned.1.call-update) | async-done | bytes 4194320 | tf_op jit(solution)/shard_map/all_gather | solution.py:18
  86.2 8.3 %fusion.8 = f32[768,1024]{1,0:T(8,128)} fusion(bf16[768,2048]{1,0:T(8,128)(2,1)} %constant_dynamic-update-slice_fusion, bf16[2048,1024]{1,0:T(8,128)(2,1)} %all-gather.3.cloned.1.call-done), kind=kOutput, calls=%fused_computation.16 | convolution fusion | flops 3221225472 | bytes 10485760 | tf_op jit(solution)/shard_map/dot_general | solution.py:22
  94.5 67.5 %all-gather.5.cloned.1.call-done = bf16[1024,2048]{1,0:T(8,128)(2,1)} async-done(((bf16[1024,256]{1,0:T(8,128)(2,1)}), bf16[1024,2048]{1,0:T(8,128)(2,1)}) %all-gather.5.cloned.1.call-update) | async-done | bytes 4194320 | tf_op jit(solution)/shard_map/all_gather | solution.py:19
  162.1 7.1 %multiply_convert_fusion = bf16[768,1024]{1,0:T(8,128)(2,1)S(1)} fusion(f32[768,1024]{1,0:T(8,128)} %fusion.8, bf16[1024,2048]{1,0:T(8,128)(2,1)} %all-gather.5.cloned.1.call-done, bf16[384,2048]{1,0:T(8,128)(2,1)} %collective-permute-done.1, bf16[384,2048]{1,0:T(8,128)(2,1)S(1)} %copy-done.3), kind=kOutput, calls=%fused_computation.8 | convolution fusion | flops 3230662656 | bytes 12058624 | tf_op jit(solution)/shard_map/dot_general | solution.py:23
  169.2 1.1 copy-done.4
  170.3 7.0 %convolution_convert_fusion = bf16[2048,1024]{1,0:T(8,128)(2,1)} fusion(bf16[768,2048]{1,0:T(8,128)(2,1)} %constant_dynamic-update-slice_fusion, bf16[768,1024]{1,0:T(8,128)(2,1)S(1)} %multiply_convert_fusion), kind=kOutput, calls=%fused_computation | convolution fusion | flops 3223322624 | bytes 8912896 | tf_op jit(solution)/shard_map/dot_general | solution.py:27
  177.4 1.3 copy-done.5
  178.7 5.3 %fusion.9 = f32[768,2048]{1,0:T(8,128)S(1)} fusion(bf16[768,1024]{1,0:T(8,128)(2,1)S(1)} %copy-done.5, bf16[2048,1024]{1,0:T(8,128)(2,1)} %all-gather.3.cloned.1.call-done), kind=kOutput, calls=%fused_computation.17 | convolution fusion | flops 3221225472 | bytes 12058624 | tf_op jit(solution)/shard_map/dot_general | solution.py:31
  184.2 1.6 collective-permute-start.2
  185.8 33.9 %collective-permute-done.2 = bf16[384,2048]{1,0:T(8,128)(2,1)S(1)} collective-permute-done((bf16[384,2048]{1,0:T(8,128)(2,1)S(1)}, bf16[384,2048]{1,0:T(8,128)(2,1)S(1)}, u32[]{:S(2)}, u32[]{:S(2)}) %collective-permute-start.2) | collective-permute-done | bytes 1572896 | tf_op jit(solution)/shard_map/ppermute | solution.py:14
  219.7 1.7 fusion
  221.4 42.5 %reduce-scatter.2.cloned.1.call-done = bf16[256,1024]{1,0:T(8,128)(2,1)} async-done(((bf16[2048,1024]{1,0:T(8,128)(2,1)}), bf16[256,1024]{1,0:T(8,128)(2,1)}) %reduce-scatter.2.cloned.1.call-update) | async-done | bytes 524304 | tf_op jit(solution)/shard_map/reduce_scatter | solution.py:30
  263.9 1.5 collective-permute-start.3
  265.6 1.2 convert_dynamic-update-slice_fusion.1
  266.8 10.8 %collective-permute-done.3 = bf16[256,1024]{1,0:T(8,128)(2,1)} collective-permute-done((bf16[256,1024]{1,0:T(8,128)(2,1)}, bf16[256,1024]{1,0:T(8,128)(2,1)}, u32[]{:S(2)}, u32[]{:S(2)}) %collective-permute-start.3) | collective-permute-done | bytes 524320 | tf_op jit(solution)/shard_map/ppermute | solution.py:14
  277.6 1.1 convert_dynamic-update-slice_fusion
  278.7 8.0 %all-reduce.2.cloned.1.call-done = bf16[384,2048]{1,0:T(8,128)(2,1)} async-done(((bf16[384,2048]{1,0:T(8,128)(2,1)}), bf16[384,2048]{1,0:T(8,128)(2,1)}) %all-reduce.2.cloned.1.call-update) | async-done | bytes 1572880 | tf_op jit(solution)/shard_map/psum | solution.py:38
  286.7 2.7 copy.10
  (22 shorter events, 1.6 us)
Async XLA Ops:
  7.2 1.2 copy-start
  7.2 4.1 %copy-start.2 = (bf16[384,2048]{1,0:T(8,128)(2,1)S(1)}, bf16[384,2048]{1,0:T(8,128)(2,1)}, u32[]{:S(2)}) copy-start(bf16[384,2048]{1,0:T(8,128)(2,1)} %param.4) | copy-start | bytes 4718596
  7.2 79.1 %all-gather.3.cloned.1.call-start = ((), (), s32[]{:S(2)}) async-start(), calls=%async_computation.1 | async-start | bytes 4718592 | tf_op jit(solution)/shard_map/all_gather | solution.py:18
  9.3 152.8 %all-gather.5.cloned.1.call-start = ((), (), s32[]{:S(2)}) async-start(), calls=%async_computation.2 | async-start | bytes 4718592 | tf_op jit(solution)/shard_map/all_gather | solution.py:19
  11.2 252.7 %reduce-scatter.2.cloned.1.call-start = ((), (), s32[]{:S(2)}) async-start(), calls=%async_computation.4 | async-start | bytes 4718592 | tf_op jit(solution)/shard_map/reduce_scatter | solution.py:30
  11.3 38.3 %collective-permute-start = (bf16[384,2048]{1,0:T(8,128)(2,1)S(1)}, bf16[384,2048]{1,0:T(8,128)(2,1)S(1)}, u32[]{:S(2)}, u32[]{:S(2)}) collective-permute-start(bf16[384,2048]{1,0:T(8,128)(2,1)S(1)} %copy-done.2), channel_id=1, source_target_pairs={{16,0},{0,16},{17,1},{1,17},{18,2},{2,18},{19,3},{3,19},{20,4},{4,... | collective-permute-start | bytes 4718600 | tf_op jit(solution)/shard_map/ppermute | solution.py:14
  14.3 80.2 %collective-permute-start.1 = (bf16[384,2048]{1,0:T(8,128)(2,1)}, bf16[384,2048]{1,0:T(8,128)(2,1)}, u32[]{:S(2)}, u32[]{:S(2)}) collective-permute-start(bf16[384,2048]{1,0:T(8,128)(2,1)} %param.7), channel_id=1, source_target_pairs={{16,0},{0,16},{17,1},{1,17},{18,2},{2,18},{19,3},{3,19},{20,4},{4,... | collective-permute-start | bytes 4718600 | tf_op jit(solution)/shard_map/ppermute | solution.py:14
  50.8 111.3 %copy-start.3 = (bf16[384,2048]{1,0:T(8,128)(2,1)S(1)}, bf16[384,2048]{1,0:T(8,128)(2,1)}, u32[]{:S(2)}) copy-start(bf16[384,2048]{1,0:T(8,128)(2,1)} %param.7) | copy-start | bytes 4718596
  169.1 1.1 copy-start.4
  177.3 1.4 copy-start.5
  177.4 109.4 %all-reduce.2.cloned.1.call-start = ((), (), s32[]{:S(2)}) async-start(), calls=%async_computation.3 | async-start | bytes 3145728 | tf_op jit(solution)/shard_map/psum | solution.py:38
  184.2 35.5 %collective-permute-start.2 = (bf16[384,2048]{1,0:T(8,128)(2,1)S(1)}, bf16[384,2048]{1,0:T(8,128)(2,1)S(1)}, u32[]{:S(2)}, u32[]{:S(2)}) collective-permute-start(bf16[384,2048]{1,0:T(8,128)(2,1)S(1)} %slice.15), channel_id=1, source_target_pairs={{16,0},{0,16},{17,1},{1,17},{18,2},{2,18},{19,3},{3,19},{20,4},{4,... | collective-permute-start | bytes 4718600 | tf_op jit(solution)/shard_map/ppermute | solution.py:14
  263.9 13.6 %collective-permute-start.3 = (bf16[256,1024]{1,0:T(8,128)(2,1)}, bf16[256,1024]{1,0:T(8,128)(2,1)}, u32[]{:S(2)}, u32[]{:S(2)}) collective-permute-start(bf16[256,1024]{1,0:T(8,128)(2,1)} %reduce-scatter.2.cloned.1.call-done), channel_id=1, source_target_pairs={{16,0},{0,16},{17,1},{1,17},{18,2},{2,18},{19,3},{3,19},{20,4},{4,... | collective-permute-start | bytes 1572872 | tf_op jit(solution)/shard_map/ppermute | solution.py:14
  278.7 10.8 %copy-start.1 = (f32[256,2048]{1,0:T(8,128)}, f32[256,2048]{1,0:T(8,128)S(1)}, u32[]{:S(2)}) copy-start(f32[256,2048]{1,0:T(8,128)S(1)} %convert_dynamic-update-slice_fusion) | copy-start | bytes 6291460
Sparse Core Ops, SparseCore 0:
  10.7 75.5 all-gather.2
  88.9 73.1 all-gather.4
  177.5 86.4 reduce-scatter.1
  266.7 19.9 all-reduce.1
where the time goes:
time: 296 us
  waiting for transfers between devices  232 us (78%)
  matrix products  27.7 us (9%)
  between operations  13.9 us (5%)
  local copies, waits for them, and re-layouts  12.1 us (4%)
  starting transfers between devices  6.32 us (2%)
  other arithmetic  4.01 us (1%)
    ppermute x4, waiting for transfers between devices, from_rep(): lax.ppermute(value, 'rep', [((r + step) % n_rep, r) for r in range(n_rep)])  78.5 us
    all_gather x1, waiting for transfers between devices, per_device(): down_whole = lax.all_gather(down_block, 'fs', axis=1, tiled=True)  67.5 us
    reduce_scatter x1, waiting for transfers between devices, per_device(): own_rows = lax.psum_scatter(d_w, 'fs', scatter_dimension=0, tiled=True)  42.5 us
    all_gather x1, waiting for transfers between devices, per_device(): up_whole = lax.all_gather(up_block, 'fs', axis=0, tiled=True)  35.4 us
    dot_general x1, matrix products, per_device(): preact = jnp.dot(rows, up_whole, preferred_element_type=jnp.float32)  8.28 us
    psum x1, waiting for transfers between devices, per_device(): d_inputs = lax.psum(own.astype(jnp.bfloat16), 'tp')  8.01 us
    unnamed x14, local copies, waits for them, and re-layouts  7.72 us
    dot_general x1, matrix products, per_device(): lax.dot_general(cots, down_whole, (((1,), (1,)), ((), ())), preferred_ele...  7.07 us
  transfers between devices with their start and end apart: 8, of which 7 were waited for; matrix products, arithmetic and copies ran while one was open for 8% of the time, Pallas kernels for 0%

commit v1 on v0

--- a/solution.py
+++ b/solution.py
@@ -15,7 +15,22 @@
 
     up_block = lax.dynamic_slice_in_dim(w_up, rep * hidden, hidden, axis=1)
     down_block = lax.dynamic_slice_in_dim(w_down, rep * hidden, hidden, axis=0)
-    up_whole = lax.all_gather(up_block, "fs", axis=0, tiled=True)
+    ways, here, step_2 = (lax.axis_size("fs"), lax.axis_index("fs"), up_block.shape[0])
+    shape = [n * ways if d == 0 else n for d, n in enumerate(up_block.shape)]
+    up_whole = lax.dynamic_update_slice_in_dim(
+        jnp.zeros(shape, up_block.dtype), up_block, here * step_2, axis=0
+    )
+    going_up = going_down = up_block
+    for far in range(1, ways // 2 + 1):
+        going_up = lax.ppermute(going_up, "fs", [(d, (d + 1) % ways) for d in range(ways)])
+        up_whole = lax.dynamic_update_slice_in_dim(
+            up_whole, going_up, (here - far) % ways * step_2, axis=0
+        )
+        if 2 * far < ways:
+            going_down = lax.ppermute(going_down, "fs", [(d, (d - 1) % ways) for d in range(ways)])
+            up_whole = lax.dynamic_update_slice_in_dim(
+                up_whole, going_down, (here + far) % ways * step_2, axis=0
+            )
     down_whole = lax.all_gather(down_block, "fs", axis=1, tiled=True)
     rows = jnp.concatenate([inputs] + [from_rep(inputs, k) for k in range(1, n_rep)], axis=0)
     cots = jnp.concatenate([cotangent] + [from_rep(cotangent, k) for k in range(1, n_rep)], axis=0)

time: 296 us -> 275 us (0.929)
  waiting for transfers between devices: 232 us -> 183 us
  starting transfers between devices: 6.32 us -> 27.5 us
  local copies, waits for them, and re-layouts: 12.1 us -> 20.9 us
    ppermute x0 -> x7, waiting for transfers between devices: none -> 79.9 us  [the longest x4 79.9 us: per_device(): lax.ppermute(going_up, 'fs', [(d, (d + 1) % ways) for d in range(ways)])]
    all_gather x1, waiting for transfers between devices: 67.5 us -> 7.15 us  [per_device(): down_whole = lax.all_gather(down_block, 'fs', axis=1, tiled=True)]
    all_gather x1 -> x0, waiting for transfers between devices: 35.4 us -> none  [per_device(): up_whole = lax.all_gather(up_block, 'fs', axis=0, tiled=True)]
    ppermute x4, waiting for transfers between devices: 78.5 us -> 45 us  [from_rep(): lax.ppermute(value, 'rep', [((r + step) % n_rep, r) for r in range(n_rep)])]
    ppermute x0 -> x7, starting transfers between devices: none -> 21.2 us  [the longest x3 13.3 us: per_device(): lax.ppermute(going_down, 'fs', [(d, (d - 1) % ways) for d in range(ways)])]
    dynamic_update_slice x0 -> x8, local copies, waits for them, and re-layouts: none -> 9.91 us  [the longest x3 4.58 us: per_device(): lax.dynamic_update_slice_in_dim(up_whole, going_down, (here + far) % ways...]
    unnamed x14 -> x18, local copies, waits for them, and re-layouts: 7.72 us -> 5.65 us
  transfers between devices with their start and end apart: 8 -> 14, of which waited for: 7 -> 9; matrix products, arithmetic and copies ran while one was open for 8% -> 12% of each run, Pallas kernels for 0% -> 0%
where the time goes in v1:
time: 275 us
  waiting for transfers between devices  183 us (67%)
  starting transfers between devices  27.5 us (10%)
  matrix products  25.7 us (9%)
  local copies, waits for them, and re-layouts  20.9 us (8%)
  between operations  13.9 us (5%)
  other arithmetic  3.94 us (1%)
    ppermute x4, waiting for transfers between devices, per_device(): lax.ppermute(going_up, 'fs', [(d, (d + 1) % ways) for d in range(ways)])  79.9 us
    ppermute x4, waiting for transfers between devices, from_rep(): lax.ppermute(value, 'rep', [((r + step) % n_rep, r) for r in range(n_rep)])  45 us
    reduce_scatter x1, waiting for transfers between devices, per_device(): own_rows = lax.psum_scatter(d_w, 'fs', scatter_dimension=0, tiled=True)  42.3 us
    ppermute x3, starting transfers between devices, per_device(): lax.ppermute(going_down, 'fs', [(d, (d - 1) % ways) for d in range(ways)])  13.3 us
    psum x1, waiting for transfers between devices, per_device(): d_inputs = lax.psum(own.astype(jnp.bfloat16), 'tp')  8.19 us
    ppermute x4, starting transfers between devices, per_device(): lax.ppermute(going_up, 'fs', [(d, (d + 1) % ways) for d in range(ways)])  7.92 us
    dot_general x1, matrix products, per_device(): preact = jnp.dot(rows, up_whole, preferred_element_type=jnp.float32)  7.32 us
    all_gather x1, waiting for transfers between devices, per_device(): down_whole = lax.all_gather(down_block, 'fs', axis=1, tiled=True)  7.15 us
  transfers between devices with their start and end apart: 14, of which 9 were waited for; matrix products, arithmetic and copies ran while one was open for 12% of the time, Pallas kernels for 0%

profile of v1, /device:TPU:0, one launch (start us, length us, event | category | flops | bytes accessed | tf_op | source)
XLA Modules:
  0.0 274.5 jit_solution(11084528928403061623)
XLA Ops:
  9.3 2.5 broadcast_in_dim.6
  12.8 3.0 %collective-permute-start.1 = (bf16[256,1024]{1,0:T(8,128)(2,1)S(1)}, bf16[256,1024]{1,0:T(8,128)(2,1)S(1)}, u32[]{:S(2)}, u32[]{:S(2)}) collective-permute-start(bf16[256,1024]{1,0:T(8,128)(2,1)S(1)} %get-tuple-element.3), channel_id=1, source_target_pairs={{0,2},{2,4},{4,6},{6,8},{8,10},{10,12},{12,14},{14,0},{1,3},{3,5},... | collective-permute-start | bytes 1572872 | tf_op jit(solution)/shard_map/ppermute | solution.py:25
  15.8 3.1 %collective-permute-start.2 = (bf16[256,1024]{1,0:T(8,128)(2,1)S(1)}, bf16[256,1024]{1,0:T(8,128)(2,1)}, u32[]{:S(2)}, u32[]{:S(2)}) collective-permute-start(bf16[256,1024]{1,0:T(8,128)(2,1)S(1)} %get-tuple-element.3), channel_id=1, source_target_pairs={{0,14},{2,0},{4,2},{6,4},{8,6},{10,8},{12,10},{14,12},{1,15},{3,1}... | collective-permute-start | bytes 1572872 | tf_op jit(solution)/shard_map/ppermute | solution.py:30
  20.5 23.3 %collective-permute-done.1 = bf16[256,1024]{1,0:T(8,128)(2,1)S(1)} collective-permute-done((bf16[256,1024]{1,0:T(8,128)(2,1)S(1)}, bf16[256,1024]{1,0:T(8,128)(2,1)S(1)}, u32[]{:S(2)}, u32[]{:S(2)}) %collective-permute-start.1) | collective-permute-done | bytes 524320 | tf_op jit(solution)/shard_map/ppermute | solution.py:25
  43.8 2.5 collective-permute-start.3
  46.3 3.1 %collective-permute-start.4 = (bf16[256,1024]{1,0:T(8,128)(2,1)}, bf16[256,1024]{1,0:T(8,128)(2,1)}, u32[]{:S(2)}, u32[]{:S(2)}) collective-permute-start(bf16[256,1024]{1,0:T(8,128)(2,1)} %collective-permute-done.2), channel_id=1, source_target_pairs={{0,14},{2,0},{4,2},{6,4},{8,6},{10,8},{12,10},{14,12},{1,15},{3,1}... | collective-permute-start | bytes 1572872 | tf_op jit(solution)/shard_map/ppermute | solution.py:30
  50.9 19.6 %collective-permute-done.3 = bf16[256,1024]{1,0:T(8,128)(2,1)} collective-permute-done((bf16[256,1024]{1,0:T(8,128)(2,1)S(1)}, bf16[256,1024]{1,0:T(8,128)(2,1)}, u32[]{:S(2)}, u32[]{:S(2)}) %collective-permute-start.3) | collective-permute-done | bytes 524320 | tf_op jit(solution)/shard_map/ppermute | solution.py:25
  70.7 7.1 %collective-permute-start.6 = (bf16[256,1024]{1,0:T(8,128)(2,1)}, bf16[256,1024]{1,0:T(8,128)(2,1)S(1)}, u32[]{:S(2)}, u32[]{:S(2)}) collective-permute-start(bf16[256,1024]{1,0:T(8,128)(2,1)} %collective-permute-done.4), channel_id=1, source_target_pairs={{0,14},{2,0},{4,2},{6,4},{8,6},{10,8},{12,10},{14,12},{1,15},{3,1}... | collective-permute-start | bytes 1572872 | tf_op jit(solution)/shard_map/ppermute | solution.py:30
  78.6 1.9 constant_dynamic-update-slice_fusion.7
  80.5 1.9 constant_dynamic-update-slice_fusion.6
  82.3 22.1 %collective-permute-done.5 = bf16[256,1024]{1,0:T(8,128)(2,1)S(1)} collective-permute-done((bf16[256,1024]{1,0:T(8,128)(2,1)}, bf16[256,1024]{1,0:T(8,128)(2,1)S(1)}, u32[]{:S(2)}, u32[]{:S(2)}) %collective-permute-start.5) | collective-permute-done | bytes 524320 | tf_op jit(solution)/shard_map/ppermute | solution.py:25
  104.4 2.4 collective-permute-start.7
  106.8 1.9 constant_dynamic-update-slice_fusion.5
  111.9 14.9 %collective-permute-done.7 = bf16[256,1024]{1,0:T(8,128)(2,1)S(1)} collective-permute-done((bf16[256,1024]{1,0:T(8,128)(2,1)S(1)}, bf16[256,1024]{1,0:T(8,128)(2,1)S(1)}, u32[]{:S(2)}, u32[]{:S(2)}) %collective-permute-start.7) | collective-permute-done | bytes 524320 | tf_op jit(solution)/shard_map/ppermute | solution.py:25
  127.6 7.3 %fusion.15 = f32[768,1024]{1,0:T(8,128)} fusion(bf16[768,2048]{1,0:T(8,128)(2,1)S(1)} %constant_dynamic-update-slice_fusion, bf16[2048,1024]{1,0:T(8,128)(2,1)} %constant_dynamic-update-slice_fusion.2), kind=kOutput, calls=%fused_computation.33 | convolution fusion | flops 3221225472 | bytes 10485760 | tf_op jit(solution)/shard_map/dot_general | solution.py:37
  134.9 7.2 %all-gather.2.cloned.1.call-done = bf16[1024,2048]{1,0:T(8,128)(2,1)} async-done(((bf16[1024,256]{1,0:T(8,128)(2,1)}), bf16[1024,2048]{1,0:T(8,128)(2,1)}) %all-gather.2.cloned.1.call-update) | async-done | bytes 4194320 | tf_op jit(solution)/shard_map/all_gather | solution.py:34
  142.1 6.3 %fusion.1 = f32[768,1024]{1,0:T(8,128)S(1)} fusion(bf16[1024,2048]{1,0:T(8,128)(2,1)} %all-gather.2.cloned.1.call-done, bf16[384,2048]{1,0:T(8,128)(2,1)} %collective-permute-done.8, bf16[384,2048]{1,0:T(8,128)(2,1)} %param.7), kind=kOutput, calls=%fused_computation.4 | convolution fusion | flops 3227516928 | bytes 10485760 | tf_op jit(solution)/shard_map/dot_general | solution.py:38
  150.1 5.2 %convolution_convert_fusion = bf16[2048,1024]{1,0:T(8,128)(2,1)} fusion(bf16[768,2048]{1,0:T(8,128)(2,1)S(1)} %copy-done.4, f32[768,1024]{1,0:T(8,128)S(1)} %fusion.1, f32[768,1024]{1,0:T(8,128)S(1)} %copy-done.6), kind=kOutput, calls=%fused_computation | convolution fusion | flops 3226468352 | bytes 13631488 | tf_op jit(solution)/shard_map/dot_general | solution.py:42
  155.4 6.9 %fusion.5 = f32[768,2048]{1,0:T(8,128)S(1)} fusion(bf16[2048,1024]{1,0:T(8,128)(2,1)} %constant_dynamic-update-slice_fusion.2, f32[768,1024]{1,0:T(8,128)} %copy-done.7, f32[768,1024]{1,0:T(8,128)} %fusion.15), kind=kOutput, calls=%fused_computation.9 | convolution fusion | flops 3224371200 | bytes 16777216 | tf_op jit(solution)/shard_map/dot_general | solution.py:46
  164.0 34.3 %collective-permute-done.9 = bf16[384,2048]{1,0:T(8,128)(2,1)S(1)} collective-permute-done((bf16[384,2048]{1,0:T(8,128)(2,1)S(1)}, bf16[384,2048]{1,0:T(8,128)(2,1)S(1)}, u32[]{:S(2)}, u32[]{:S(2)}) %collective-permute-start.9) | collective-permute-done | bytes 1572896 | tf_op jit(solution)/shard_map/ppermute | solution.py:14
  200.0 42.3 %reduce-scatter.2.cloned.1.call-done = bf16[256,1024]{1,0:T(8,128)(2,1)} async-done(((bf16[2048,1024]{1,0:T(8,128)(2,1)}), bf16[256,1024]{1,0:T(8,128)(2,1)}) %reduce-scatter.2.cloned.1.call-update) | async-done | bytes 524304 | tf_op jit(solution)/shard_map/reduce_scatter | solution.py:45
  245.2 10.7 %collective-permute-done.10 = bf16[256,1024]{1,0:T(8,128)(2,1)} collective-permute-done((bf16[256,1024]{1,0:T(8,128)(2,1)}, bf16[256,1024]{1,0:T(8,128)(2,1)}, u32[]{:S(2)}, u32[]{:S(2)}) %collective-permute-start.10) | collective-permute-done | bytes 524320 | tf_op jit(solution)/shard_map/ppermute | solution.py:14
  257.1 8.2 %all-reduce.2.cloned.1.call-done = bf16[384,2048]{1,0:T(8,128)(2,1)} async-done(((bf16[384,2048]{1,0:T(8,128)(2,1)}), bf16[384,2048]{1,0:T(8,128)(2,1)}) %all-reduce.2.cloned.1.call-update) | async-done | bytes 1572880 | tf_op jit(solution)/shard_map/psum | solution.py:53
  265.3 2.7 copy.18
  (45 shorter events, 20.4 us)
Async XLA Ops:
  7.2 1.2 copy-start
  7.2 134.9 %all-gather.2.cloned.1.call-start = ((), (), s32[]{:S(2)}) async-start(), calls=%async_computation.1 | async-start | bytes 4718592 | tf_op jit(solution)/shard_map/all_gather | solution.py:34
  9.2 9.6 %copy-start.2 = (bf16[384,2048]{1,0:T(8,128)(2,1)S(1)}, bf16[384,2048]{1,0:T(8,128)(2,1)}, u32[]{:S(2)}) copy-start(bf16[384,2048]{1,0:T(8,128)(2,1)} %param.4) | copy-start | bytes 4718596
  9.2 233.1 %reduce-scatter.2.cloned.1.call-start = ((), (), s32[]{:S(2)}) async-start(), calls=%async_computation.3 | async-start | bytes 4718592 | tf_op jit(solution)/shard_map/reduce_scatter | solution.py:45
  9.3 2.6 copy-start.5
  12.8 31.0 %collective-permute-start.1 = (bf16[256,1024]{1,0:T(8,128)(2,1)S(1)}, bf16[256,1024]{1,0:T(8,128)(2,1)S(1)}, u32[]{:S(2)}, u32[]{:S(2)}) collective-permute-start(bf16[256,1024]{1,0:T(8,128)(2,1)S(1)} %get-tuple-element.3), channel_id=1, source_target_pairs={{0,2},{2,4},{4,6},{6,8},{8,10},{10,12},{12,14},{14,0},{1,3},{3,5},... | collective-permute-start | bytes 1572872 | tf_op jit(solution)/shard_map/ppermute | solution.py:25
  15.8 30.5 %collective-permute-start.2 = (bf16[256,1024]{1,0:T(8,128)(2,1)S(1)}, bf16[256,1024]{1,0:T(8,128)(2,1)}, u32[]{:S(2)}, u32[]{:S(2)}) collective-permute-start(bf16[256,1024]{1,0:T(8,128)(2,1)S(1)} %get-tuple-element.3), channel_id=1, source_target_pairs={{0,14},{2,0},{4,2},{6,4},{8,6},{10,8},{12,10},{14,12},{1,15},{3,1}... | collective-permute-start | bytes 1572872 | tf_op jit(solution)/shard_map/ppermute | solution.py:30
  18.9 91.5 %collective-permute-start = (bf16[384,2048]{1,0:T(8,128)(2,1)S(1)}, bf16[384,2048]{1,0:T(8,128)(2,1)}, u32[]{:S(2)}, u32[]{:S(2)}) collective-permute-start(bf16[384,2048]{1,0:T(8,128)(2,1)S(1)} %copy-done.2), channel_id=1, source_target_pairs={{16,0},{0,16},{17,1},{1,17},{18,2},{2,18},{19,3},{3,19},{20,4},{4,... | collective-permute-start | bytes 4718600 | tf_op jit(solution)/shard_map/ppermute | solution.py:14
  43.8 26.6 %collective-permute-start.3 = (bf16[256,1024]{1,0:T(8,128)(2,1)S(1)}, bf16[256,1024]{1,0:T(8,128)(2,1)}, u32[]{:S(2)}, u32[]{:S(2)}) collective-permute-start(bf16[256,1024]{1,0:T(8,128)(2,1)S(1)} %collective-permute-done.1), channel_id=1, source_target_pairs={{0,2},{2,4},{4,6},{6,8},{8,10},{10,12},{12,14},{14,0},{1,3},{3,5},... | collective-permute-start | bytes 1572872 | tf_op jit(solution)/shard_map/ppermute | solution.py:25
  46.3 24.4 %collective-permute-start.4 = (bf16[256,1024]{1,0:T(8,128)(2,1)}, bf16[256,1024]{1,0:T(8,128)(2,1)}, u32[]{:S(2)}, u32[]{:S(2)}) collective-permute-start(bf16[256,1024]{1,0:T(8,128)(2,1)} %collective-permute-done.2), channel_id=1, source_target_pairs={{0,14},{2,0},{4,2},{6,4},{8,6},{10,8},{12,10},{14,12},{1,15},{3,1}... | collective-permute-start | bytes 1572872 | tf_op jit(solution)/shard_map/ppermute | solution.py:30
  49.4 85.6 %collective-permute-start.8 = (bf16[384,2048]{1,0:T(8,128)(2,1)}, bf16[384,2048]{1,0:T(8,128)(2,1)}, u32[]{:S(2)}, u32[]{:S(2)}) collective-permute-start(bf16[384,2048]{1,0:T(8,128)(2,1)} %param.7), channel_id=1, source_target_pairs={{16,0},{0,16},{17,1},{1,17},{18,2},{2,18},{19,3},{3,19},{20,4},{4,... | collective-permute-start | bytes 4718600 | tf_op jit(solution)/shard_map/ppermute | solution.py:14
  70.4 34.0 %collective-permute-start.5 = (bf16[256,1024]{1,0:T(8,128)(2,1)}, bf16[256,1024]{1,0:T(8,128)(2,1)S(1)}, u32[]{:S(2)}, u32[]{:S(2)}) collective-permute-start(bf16[256,1024]{1,0:T(8,128)(2,1)} %collective-permute-done.3), channel_id=1, source_target_pairs={{0,2},{2,4},{4,6},{6,8},{8,10},{10,12},{12,14},{14,0},{1,3},{3,5},... | collective-permute-start | bytes 1572872 | tf_op jit(solution)/shard_map/ppermute | solution.py:25
  70.7 38.8 %collective-permute-start.6 = (bf16[256,1024]{1,0:T(8,128)(2,1)}, bf16[256,1024]{1,0:T(8,128)(2,1)S(1)}, u32[]{:S(2)}, u32[]{:S(2)}) collective-permute-start(bf16[256,1024]{1,0:T(8,128)(2,1)} %collective-permute-done.4), channel_id=1, source_target_pairs={{0,14},{2,0},{4,2},{6,4},{8,6},{10,8},{12,10},{14,12},{1,15},{3,1}... | collective-permute-start | bytes 1572872 | tf_op jit(solution)/shard_map/ppermute | solution.py:30
  104.4 22.4 %collective-permute-start.7 = (bf16[256,1024]{1,0:T(8,128)(2,1)S(1)}, bf16[256,1024]{1,0:T(8,128)(2,1)S(1)}, u32[]{:S(2)}, u32[]{:S(2)}) collective-permute-start(bf16[256,1024]{1,0:T(8,128)(2,1)S(1)} %collective-permute-done.5), channel_id=1, source_target_pairs={{0,2},{2,4},{4,6},{6,8},{8,10},{10,12},{12,14},{14,0},{1,3},{3,5},... | collective-permute-start | bytes 1572872 | tf_op jit(solution)/shard_map/ppermute | solution.py:25
  111.9 23.1 %copy-start.3 = (bf16[768,2048]{1,0:T(8,128)(2,1)}, bf16[768,2048]{1,0:T(8,128)(2,1)S(1)}, u32[]{:S(2)}) copy-start(bf16[768,2048]{1,0:T(8,128)(2,1)S(1)} %constant_dynamic-update-slice_fusion) | copy-start | bytes 9437188
  142.1 8.0 %copy-start.4 = (bf16[768,2048]{1,0:T(8,128)(2,1)S(1)}, bf16[768,2048]{1,0:T(8,128)(2,1)}, u32[]{:S(2)}) copy-start(bf16[768,2048]{1,0:T(8,128)(2,1)} %copy-done.3) | copy-start | bytes 9437188
  142.1 8.0 %copy-start.6 = (f32[768,1024]{1,0:T(8,128)S(1)}, f32[768,1024]{1,0:T(8,128)}, u32[]{:S(2)}) copy-start(f32[768,1024]{1,0:T(8,128)} %fusion.15) | copy-start | bytes 9437188
  148.5 1.6 copy-start.7
  155.3 109.9 %all-reduce.2.cloned.1.call-start = ((), (), s32[]{:S(2)}) async-start(), calls=%async_computation.2 | async-start | bytes 3145728 | tf_op jit(solution)/shard_map/psum | solution.py:53
  162.5 35.9 %collective-permute-start.9 = (bf16[384,2048]{1,0:T(8,128)(2,1)S(1)}, bf16[384,2048]{1,0:T(8,128)(2,1)S(1)}, u32[]{:S(2)}, u32[]{:S(2)}) collective-permute-start(bf16[384,2048]{1,0:T(8,128)(2,1)S(1)} %slice.15), channel_id=1, source_target_pairs={{16,0},{0,16},{17,1},{1,17},{18,2},{2,18},{19,3},{3,19},{20,4},{4,... | collective-permute-start | bytes 4718600 | tf_op jit(solution)/shard_map/ppermute | solution.py:14
  242.3 13.6 %collective-permute-start.10 = (bf16[256,1024]{1,0:T(8,128)(2,1)}, bf16[256,1024]{1,0:T(8,128)(2,1)}, u32[]{:S(2)}, u32[]{:S(2)}) collective-permute-start(bf16[256,1024]{1,0:T(8,128)(2,1)} %reduce-scatter.2.cloned.1.call-done), channel_id=1, source_target_pairs={{16,0},{0,16},{17,1},{1,17},{18,2},{2,18},{19,3},{3,19},{20,4},{4,... | collective-permute-start | bytes 1572872 | tf_op jit(solution)/shard_map/ppermute | solution.py:14
  257.1 10.9 %copy-start.1 = (f32[256,2048]{1,0:T(8,128)}, f32[256,2048]{1,0:T(8,128)S(1)}, u32[]{:S(2)}) copy-start(f32[256,2048]{1,0:T(8,128)S(1)} %convert_dynamic-update-slice_fusion) | copy-start | bytes 6291460
Sparse Core Ops, SparseCore 0:
  10.6 131.4 all-gather.1
  155.5 86.8 reduce-scatter.1
  245.2 19.9 all-reduce.1
